TPU v7x, 32 devices: a whole 2x2x4 slice. The times are simulated.
32 devices in a mesh: fs: 8 (over z, core), tp: 4 (over y, x).
Axes of the slice: x: 2, y: 2, z: 4, core: 2. Of those that a mesh axis runs over, the one named last changes fastest.
Arguments:
- latent: bfloat16 [16384, 1024], P('fs'), may hold values from -6 to 6
- key_cotangent: bfloat16 [16384, 512], P('fs', 'tp'), may hold values from -0.046875 to 0.046875
- value_cotangent: bfloat16 [16384, 512], P('fs', 'tp'), may hold values from -0.046875 to 0.046875
- key_weight: float32 [1024, 512], P('fs', 'tp'), may hold values from -50 to 50
- value_weight: float32 [1024, 512], P('fs', 'tp'), may hold values from -50 to 50
- key_projector: bfloat16 [1024, 256], replicated, may hold values from -0.1875 to 0.1875
- value_projector: bfloat16 [1024, 256], replicated, may hold values from -0.1875 to 0.1875
- key_first: float32 [256, 512], P(None, 'tp'), may hold values from -6 to 6
- key_second: float32 [256, 512], P(None, 'tp'), may hold values from 0.3 to 3
- value_first: float32 [256, 512], P(None, 'tp'), may hold values from -6 to 6
- value_second: float32 [256, 512], P(None, 'tp'), may hold values from 0.3 to 3
Outputs:
- key_renewed: float32 [1024, 512], P('fs', 'tp')
- value_renewed: float32 [1024, 512], P('fs', 'tp')
- key_step: float32 [1024, 512], P('fs', 'tp')
- value_step: float32 [1024, 512], P('fs', 'tp')
- key_first_new: float32 [256, 512], P(None, 'tp')
- key_second_new: float32 [256, 512], P(None, 'tp')
- value_first_new: float32 [256, 512], P(None, 'tp')
- value_second_new: float32 [256, 512], P(None, 'tp')
- key_copy: bfloat16 [1024, 512], P(None, 'tp')
- value_copy: bfloat16 [1024, 512], P(None, 'tp')
All inputs are finite; a program needn't handle non-finite values.
Results may differ from a plain program's by a relative error of at most 0.015.
Values may be sent and summed in bfloat16 or wider, within the bound.
A program may use at most 64 MiB of HBM per device.

v0:
```python
import functools

import jax
import jax.numpy as jnp
from jax import lax
from jax.experimental import pallas as pl
from jax.experimental.pallas import tpu as pltpu
from jax.sharding import PartitionSpec as P

EPSILON = 1e-08
FIRST_DECAY = 0.7
SECOND_DECAY = 0.8
LEARN_RATE = 0.2
CHUNKS = 4
MESH = pl.DeviceIdType.MESH
HBM = pl.BlockSpec(memory_space=pltpu.MemorySpace.HBM)
VMEM = pl.BlockSpec(memory_space=pltpu.MemorySpace.VMEM)


def exchange_kernel(
    n,
    m,
    latent,
    key_cot,
    value_cot,
    key_weight,
    value_weight,
    key_proj,
    value_proj,
    key_first,
    key_second,
    value_first,
    value_second,
    gathered,
    weights,
    squares,
    weight_v,
    proj_v,
    moment_v,
    latent_v,
    cot_v,
    cot_t,
    partial,
    received,
    tp_squares,
    load_sem,
    latent_sem,
    rs_send,
    rs_recv,
    ag_send,
    ag_recv,
    w_send,
    w_recv,
    f_send,
    f_recv,
    t_send,
    t_recv,
    s_send,
    s_recv,
):
    me = lax.axis_index("fs")
    mine = lax.axis_index("tp")
    core = lax.rem(me, 2)
    partner = me + 1 - 2 * core
    half = n // 2
    tokens, width = latent.shape
    step = width // CHUNKS
    rank = key_proj.shape[1]
    cols = key_cot.shape[1]
    piece = partial.shape[0] // n
    f32, bf16 = jnp.float32, jnp.bfloat16

    loads = [
        pltpu.make_async_copy(src, dst, load_sem.at[i])
        for i, (src, dst) in enumerate(
            (
                (key_weight, weight_v.at[0]),
                (value_weight, weight_v.at[1]),
                (key_cot, cot_v.at[0]),
                (value_cot, cot_v.at[1]),
                (key_proj, proj_v.at[0]),
                (value_proj, proj_v.at[1]),
                (key_first, moment_v.at[0]),
                (key_second, moment_v.at[1]),
                (value_first, moment_v.at[2]),
                (value_second, moment_v.at[3]),
            )
        )
    ]
    streams = [
        pltpu.make_async_copy(
            latent.at[:, pl.ds(c * step, step)], latent_v.at[c], latent_sem.at[c]
        )
        for c in range(CHUNKS)
    ]
    for copy in loads[:4]:
        copy.start()
    streams[0].start()
    for copy in loads[4:6]:
        copy.start()
    for copy in streams[1:]:
        copy.start()
    for copy in loads[6:]:
        copy.start()

    barrier = pltpu.get_barrier_semaphore()
    for d in range(1, n):
        pl.semaphore_signal(
            barrier, inc=1, device_id={"fs": lax.rem(me + d, n)}, device_id_type=MESH
        )
    for d in range(1, m):
        pl.semaphore_signal(
            barrier, inc=1, device_id={"tp": lax.rem(mine + d, m)}, device_id_type=MESH
        )

    def send(src, dst, send_sem, recv_sem, where):
        copy = pltpu.make_async_remote_copy(
            src_ref=src,
            dst_ref=dst,
            send_sem=send_sem,
            recv_sem=recv_sem,
            device_id=where,
            device_id_type=MESH,
        )
        copy.start()
        return copy

    def arrived(ref, sem):
        pltpu.make_async_remote_copy(
            src_ref=ref,
            dst_ref=ref,
            send_sem=sem,
            recv_sem=sem,
            device_id={"fs": partner},
            device_id_type=MESH,
        ).wait_recv()

    chip = lax.div(me, 2)
    side = lax.div(chip, (half + 1) // 2)

    def far_first(k):
        down = half - 1 - k
        down = down - lax.div(chip - down + half, half)
        up = k + lax.div(k - chip + half, half)
        return down + side * (up - down)

    def peers():
        for k in range(half - 1):
            base = 2 * far_first(k)
            yield base + 1 - core
            yield base + core
        yield partner

    sent = []
    loads[0].wait()
    loads[1].wait()
    for i in range(2):
        w = weight_v[i]
        weights[me, i] = w.astype(bf16)
        tp_squares[mine, pl.ds(i, 1), :] = jnp.sum(w * w, axis=0, keepdims=True)
    loads[2].wait()
    loads[3].wait()
    for i in range(2):
        cot_t[pl.ds(i * cols, cols), :] = cot_v[i].T

    pl.semaphore_wait(barrier, n - 1 + m - 1)

    def send_weights(d):
        sent.append(
            send(
                weights.at[me],
                weights.at[me],
                w_send.at[d],
                w_recv.at[me],
                {"fs": 2 * far_first(d - 1) + core},
            )
        )

    for d in range(1, m):
        sent.append(
            send(
                tp_squares.at[mine],
                tp_squares.at[mine],
                t_send.at[d],
                t_recv.at[mine],
                {"tp": lax.rem(mine + d, m)},
            )
        )
    sent.append(
        send(
            weights.at[me], weights.at[me], f_send.at[0], f_recv.at[me], {"fs": partner}
        )
    )
    for d in range(1, half):
        send_weights(d)

    totals = [None, None]
    for c in range(CHUNKS):
        streams[c].wait()
        g = jnp.dot(cot_t[...], latent_v[c], preferred_element_type=f32).astype(bf16)
        if c == 0:
            loads[4].wait()
            loads[5].wait()
        for i in range(2):
            term = jnp.dot(
                g[i * cols : (i + 1) * cols],
                proj_v[i, pl.ds(c * step, step), :],
                preferred_element_type=f32,
            )
            totals[i] = term if totals[i] is None else totals[i] + term
    for i in range(2):
        partial[pl.ds(i * rank, rank), :] = totals[i].T.astype(bf16)

    for d in range(1, m):
        arrived(tp_squares.at[lax.rem(mine + d, m)], t_recv.at[lax.rem(mine + d, m)])
    squares[me] = jnp.sum(tp_squares[...], axis=0)

    for d, peer in enumerate(peers()):
        sent.append(
            send(
                partial.at[pl.ds(peer * piece, piece)],
                received.at[me],
                rs_send.at[d],
                rs_recv.at[me],
                {"fs": peer},
            )
        )
    received[me] = partial[pl.ds(pl.multiple_of(me * piece, piece), piece), :]
    for d in range(1, n):
        sent.append(
            send(
                squares.at[me],
                squares.at[me],
                s_send.at[d],
                s_recv.at[me],
                {"fs": lax.rem(me + d, n)},
            )
        )
    for d in range(1, n):
        peer = lax.rem(me + d, n)
        arrived(received.at[peer], rs_recv.at[peer])
    gathered[me] = jnp.sum(received[...].astype(f32), axis=0).astype(bf16)
    for d, peer in enumerate(peers()):
        sent.append(
            send(
                gathered.at[me],
                gathered.at[me],
                ag_send.at[d],
                ag_recv.at[me],
                {"fs": peer},
            )
        )
    for d in range(1, half):
        source = lax.rem(me + 2 * d, n)
        arrived(weights.at[source], w_recv.at[source])
        sent.append(
            send(
                weights.at[source],
                weights.at[source],
                f_send.at[d],
                f_recv.at[source],
                {"fs": partner},
            )
        )
    for d in range(half):
        source = lax.rem(partner + 2 * d, n)
        arrived(weights.at[source], f_recv.at[source])
    for d in range(1, n):
        peer = lax.rem(me + d, n)
        arrived(squares.at[peer], s_recv.at[peer])
    for d in range(1, n):
        peer = lax.rem(me + d, n)
        arrived(gathered.at[peer], ag_recv.at[peer])
    for copy in loads[6:]:
        copy.wait()
    for copy in sent:
        copy.wait_send()


def update_kernel(n, entries, *refs):
    gathered, weights, squares, weight_v, proj_v, moment_v = refs[:6]
    outs, stage, sems = refs[6:16], refs[16:26], refs[26]
    me = lax.axis_index("fs")
    f32, bf16 = jnp.float32, jnp.bfloat16
    parts = n // 2
    rows, cols = weight_v.shape[1:]
    rank = moment_v.shape[1]
    copies = [
        pltpu.make_async_copy(src, dst, sems.at[i])
        for i, (src, dst) in enumerate(zip(stage, outs))
    ]
    normalized = []
    for i in range(2):
        projected = (
            gathered[i * parts : (i + 1) * parts].astype(f32).reshape(rank, cols)
        )
        first_new = FIRST_DECAY * moment_v[2 * i] + (1.0 - FIRST_DECAY) * projected
        second_new = (
            SECOND_DECAY * moment_v[2 * i + 1]
            + (1.0 - SECOND_DECAY) * projected * projected
        )
        stage[4 + 2 * i][...] = first_new
        stage[5 + 2 * i][...] = second_new
        copies[4 + 2 * i].start()
        copies[5 + 2 * i].start()
        normalized.append((first_new / (jnp.sqrt(second_new) + EPSILON)).astype(bf16))
    tile = jnp.sum(squares[...], axis=0)
    for i in range(2):
        total = jnp.sum(tile[i : i + 1], keepdims=True)
        scale = LEARN_RATE * jnp.sqrt(total / entries)
        every = scale * jnp.dot(proj_v[i], normalized[i], preferred_element_type=f32)
        held = weights[:, i].astype(f32).reshape(n * rows, cols)
        stage[8 + i][...] = (held - every).astype(bf16)
        copies[8 + i].start()
        own = proj_v[i, pl.ds(pl.multiple_of(me * rows, rows), rows), :]
        own_step = scale * jnp.dot(own, normalized[i], preferred_element_type=f32)
        stage[2 + i][...] = own_step
        stage[i][...] = weight_v[i] - own_step
        copies[2 + i].start()
        copies[i].start()
    for copy in copies:
        copy.wait()


def solution(mesh):
    n, m = mesh.shape["fs"], mesh.shape["tp"]

    def body(
        latent,
        key_cot,
        value_cot,
        key_weight,
        value_weight,
        key_proj,
        value_proj,
        key_first,
        key_second,
        value_first,
        value_second,
    ):
        f32, bf16 = jnp.float32, jnp.bfloat16
        sds = jax.ShapeDtypeStruct
        tokens, width = latent.shape
        rows, cols = key_weight.shape
        rank = key_proj.shape[1]
        piece = 2 * rank // n
        dma = pltpu.SemaphoreType.DMA
        held = pl.pallas_call(
            functools.partial(exchange_kernel, n, m),
            out_shape=(
                sds((n, piece, cols), bf16),
                sds((n, 2, rows, cols), bf16),
                sds((n, 2, cols), f32),
                sds((2, rows, cols), f32),
                sds((2, width, rank), bf16),
                sds((4, rank, cols), f32),
            ),
            in_specs=[HBM] * 11,
            out_specs=(VMEM,) * 6,
            scratch_shapes=[
                pltpu.VMEM((CHUNKS, tokens, width // CHUNKS), bf16),
                pltpu.VMEM((2, tokens, cols), bf16),
                pltpu.VMEM((2 * cols, tokens), bf16),
                pltpu.VMEM((2 * rank, cols), bf16),
                pltpu.VMEM((n, piece, cols), bf16),
                pltpu.VMEM((m, 2, cols), f32),
                dma((10,)),
                dma((CHUNKS,)),
                dma((n,)),
                dma((n,)),
                dma((n,)),
                dma((n,)),
                dma((n,)),
                dma((n,)),
                dma((n,)),
                dma((n,)),
                dma((m,)),
                dma((m,)),
                dma((n,)),
                dma((n,)),
            ],
            compiler_params=pltpu.CompilerParams(
                collective_id=0, has_side_effects=True, vmem_limit_bytes=24 << 20
            ),
        )(
            *(
                pltpu.with_memory_space_constraint(x, pltpu.MemorySpace.HBM)
                for x in (
                    latent,
                    key_cot,
                    value_cot,
                    key_weight,
                    value_weight,
                    key_proj,
                    value_proj,
                    key_first,
                    key_second,
                    value_first,
                    value_second,
                )
            )
        )
        small = sds((rows, cols), f32)
        moment = sds((rank, cols), f32)
        copy = sds((n * rows, cols), bf16)
        return pl.pallas_call(
            functools.partial(update_kernel, n, float(rows * cols * n * m)),
            out_shape=(small,) * 4 + (moment,) * 4 + (copy,) * 2,
            in_specs=[VMEM] * 6,
            out_specs=(HBM,) * 10,
            scratch_shapes=[pltpu.VMEM((rows, cols), f32)] * 4
            + [pltpu.VMEM((rank, cols), f32)] * 4
            + [pltpu.VMEM((n * rows, cols), bf16)] * 2
            + [dma((10,))],
            compiler_params=pltpu.CompilerParams(vmem_limit_bytes=24 << 20),
        )(*held)

    split, column = P("fs", "tp"), P(None, "tp")
    return jax.shard_map(
        body,
        mesh=mesh,
        in_specs=(P("fs", None),) + (split,) * 4 + (P(),) * 2 + (column,) * 4,
        out_specs=(split,) * 4 + (column,) * 6,
        check_vma=False,
    )
```

profile of v0, /device:TPU:0, one launch (start us, length us, event | category | flops | bytes accessed | tf_op | source)
XLA Modules:
  0.0 22.6 jit_solution(13489336780644520437)
XLA Ops:
  0.6 20.4 %shard_map.186 = (bf16[8,64,128]{2,1,0:T(8,128)(2,1)S(1)}, bf16[8,2,128,128]{3,2,1,0:T(8,128)(2,1)S(1)}, f32[8,2,128]{2,1,0:T(2,128)S(1)}, f32[2,128,128]{2,1,0:...) custom-call(bf16[2048,1024]{1,0:T(8,128)(2,1)} %latent.1, bf16[2048,128]{1,0:T(8,128)(2,1)} %key_cot.1, ...), custom_call_target="tpu_custom_call" | custom-call | tf_op jit(solution)/shard_map/pallas_call | solution.py:348
  21.1 1.5 %shard_map.187 = (f32[128,128]{1,0:T(8,128)}, f32[128,128]{1,0:T(8,128)}, f32[128,128]{1,0:T(8,128)}, f32[128,128]{1,0:T(8,128)}, f32[256,128]{1,0:T(8,128)}, /*...) custom-call(bf16[8,64,128]{2,1,0:T(8,128)(2,1)S(1)} %get-tuple-eleme, ...), custom_call_target="tpu_custom_call" | custom-call | tf_op jit(solution)/shard_map/pallas_call | solution.py:406
where the time goes:
time: 22.8 us; the launch traced here: 22.6 us
  Pallas kernels  21.9 us (96%)
  between operations  0.65 us (3%)
    pallas_call x1, Pallas kernels, body(): pl.pallas_call(functools.partial(exchange_kernel, n, m), out_shape=(sds((...  20.4 us
    pallas_call x1, Pallas kernels, body(): pl.pallas_call(functools.partial(update_kernel, n, float(rows * cols * n...  1.51 us

commit v1 on v0

v1 whole, which is shorter than its diff:
```python
import functools

import jax
import jax.numpy as jnp
from jax import lax
from jax.experimental import pallas as pl
from jax.experimental.pallas import tpu as pltpu
from jax.sharding import PartitionSpec as P

EPSILON = 1e-08
FIRST_DECAY = 0.7
SECOND_DECAY = 0.8
LEARN_RATE = 0.2
CHUNKS = 4
BARRIER_CHUNK = 3
MESH = pl.DeviceIdType.MESH
HBM = pl.BlockSpec(memory_space=pltpu.MemorySpace.HBM)
VMEM = pl.BlockSpec(memory_space=pltpu.MemorySpace.VMEM)


def exchange_kernel(
    n,
    m,
    latent,
    key_cot,
    value_cot,
    key_weight,
    value_weight,
    key_proj,
    value_proj,
    key_first,
    key_second,
    value_first,
    value_second,
    gathered,
    weights,
    squares,
    weight_v,
    proj_v,
    moment_v,
    latent_v,
    cot_v,
    cot_t,
    reduced,
    partial,
    joined,
    received,
    tp_squares,
    load_sem,
    latent_sem,
    t_send,
    t_recv,
    s_send,
    s_recv,
    c_send,
    c_recv,
    rs_send,
    rs_recv,
    ag_send,
    ag_recv,
    p_send,
    p_recv,
    x_send,
    x_recv,
    w_send,
    w_recv,
    r_send,
    f_send,
    f_recv,
):
    me = lax.axis_index("fs")
    mine = lax.axis_index("tp")
    core = lax.rem(me, 2)
    chip = lax.div(me, 2)
    partner = me + 1 - 2 * core
    half = n // 2
    tokens, width = latent.shape
    step = width // CHUNKS
    rank = key_proj.shape[1]
    cols = key_cot.shape[1]
    piece = gathered.shape[1]
    f32, bf16 = jnp.float32, jnp.bfloat16

    def load(src, dst, sem):
        pltpu.make_async_copy(src, dst, sem).start()

    def landed(ref, sem):
        pltpu.make_async_copy(ref, ref, sem).wait()

    load(key_cot, cot_v.at[0], load_sem.at[0])
    load(value_cot, cot_v.at[1], load_sem.at[0])
    load(key_weight, weight_v.at[0], load_sem.at[1])
    load(value_weight, weight_v.at[1], load_sem.at[1])
    for c in range(CHUNKS):
        load(latent.at[:, pl.ds(c * step, step)], latent_v.at[c], latent_sem.at[c])
    load(key_proj, proj_v.at[0], load_sem.at[2])
    load(value_proj, proj_v.at[1], load_sem.at[2])
    load(key_first, moment_v.at[0], load_sem.at[3])
    load(key_second, moment_v.at[1], load_sem.at[3])
    load(value_first, moment_v.at[2], load_sem.at[3])
    load(value_second, moment_v.at[3], load_sem.at[3])

    barrier = pltpu.get_barrier_semaphore()
    for d in range(1, n):
        pl.semaphore_signal(
            barrier, inc=1, device_id={"fs": lax.rem(me + d, n)}, device_id_type=MESH
        )
    for d in range(1, m):
        pl.semaphore_signal(
            barrier, inc=1, device_id={"tp": lax.rem(mine + d, m)}, device_id_type=MESH
        )

    def remote(src, dst, send_sem, recv_sem, where):
        return pltpu.make_async_remote_copy(
            src_ref=src,
            dst_ref=dst,
            send_sem=send_sem,
            recv_sem=recv_sem,
            device_id=where,
            device_id_type=MESH,
        )

    def send(src, dst, send_sem, recv_sem, where):
        remote(src, dst, send_sem, recv_sem, where).start()

    def arrived(ref, sem):
        remote(ref, ref, sem, sem, {"fs": partner}).wait_recv()

    def left(ref, sem):
        remote(ref, ref, sem, sem, {"fs": partner}).wait_send()

    side = lax.div(chip, (half + 1) // 2)

    def far_first(k):
        down = half - 1 - k
        down = down - lax.div(chip - down + half, half)
        up = k + lax.div(k - chip + half, half)
        return down + side * (up - down)

    def near_first(k):
        return far_first(half - 2 - k)

    def direct(target):
        inner = (target > 0) & (target < half - 1)
        low = (target == 0) & (chip == 1)
        high = (target == half - 1) & (chip == half - 2)
        return inner | low | high

    def spread(shard):
        for k in range(half - 1):
            target = far_first(k)

            @pl.when(direct(target))
            def _():
                send(
                    weights.at[shard],
                    weights.at[shard],
                    w_send,
                    w_recv.at[shard],
                    {"fs": 2 * target},
                )

    with jax.named_scope("cot"):
        landed(cot_v, load_sem.at[0])
    for i in range(2):
        cot_t[pl.ds(i * cols, cols), :] = cot_v[i].T
    landed(weight_v, load_sem.at[1])
    for i in range(2):
        w = weight_v[i]
        weights[me, i] = w.astype(bf16)
        tp_squares[mine, pl.ds(i, 1), :] = jnp.sum(w * w, axis=0, keepdims=True)

    for c in range(CHUNKS):
        if c == BARRIER_CHUNK:
            with jax.named_scope("bar"):
                pl.semaphore_wait(barrier, n - 1 + m - 1)
            for d in range(1, m):
                send(
                    tp_squares.at[mine],
                    tp_squares.at[mine],
                    t_send,
                    t_recv,
                    {"tp": lax.rem(mine + d, m)},
                )
            send(weights.at[me], weights.at[me], x_send, x_recv, {"fs": partner})

            @pl.when(core == 0)
            def _():
                spread(me)

        with jax.named_scope(f"lat{c}"):
            landed(latent_v.at[c], latent_sem.at[c])
        reduced[:, pl.ds(c * step, step)] = jnp.dot(
            cot_t[...], latent_v[c], preferred_element_type=f32
        ).astype(bf16)
    landed(proj_v, load_sem.at[2])
    totals = [
        jnp.dot(
            reduced[pl.ds(i * cols, cols), :], proj_v[i], preferred_element_type=f32
        ).T
        for i in range(2)
    ]

    def spread_squares():
        for_all = [lax.rem(mine + d, m) for d in range(1, m)]
        arrived(tp_squares.at[pl.ds(0, len(for_all))], t_recv)
        squares[me] = jnp.sum(tp_squares[...], axis=0)
        for d in range(1, n):
            send(
                squares.at[me],
                squares.at[me],
                s_send,
                s_recv,
                {"fs": lax.rem(me + d, n)},
            )

    @pl.when(core == 0)
    def _():
        for i in range(2):
            partial[pl.ds(i * rank, rank), :] = totals[i].astype(bf16)
        send(partial, joined, c_send, c_recv, {"fs": partner})
        with jax.named_scope("xw"):
            arrived(weights.at[partner], x_recv)
        spread(partner)
        with jax.named_scope("tpsq"):
            spread_squares()
        for part in range(2):
            for k in range(half - 1):
                source = 2 * near_first(k) + part
                with jax.named_scope(f"w{part}{k}"):
                    arrived(weights.at[source], w_recv.at[source])
                for end, next_to_end in ((0, 1), (half - 1, half - 2)):

                    @pl.when((chip == next_to_end) & (lax.div(source, 2) != end))
                    def _():
                        send(
                            weights.at[source],
                            weights.at[source],
                            r_send,
                            w_recv.at[source],
                            {"fs": 2 * end},
                        )

                send(
                    weights.at[source],
                    weights.at[source],
                    f_send,
                    f_recv,
                    {"fs": partner},
                )
        with jax.named_scope("final"):
            arrived(gathered, p_recv)
        left(partial, c_send)
        for c in range(half):
            others = [t for t in range(half) if t != c]
            count = sum(
                0 < t < half - 1
                or (t == 0 and c == 1)
                or (t == half - 1 and c == half - 2)
                for t in others
            )
            ends = (0, 1), (half - 1, half - 2)
            relays = sum(t != end for end, near in ends if near == c for t in others)

            @pl.when(chip == c)
            def _():
                if count:
                    left(weights.at[pl.ds(0, 2 * count)], w_send)
                if relays:
                    left(weights.at[pl.ds(0, 2 * relays)], r_send)

        left(weights.at[pl.ds(0, n - 2)], f_send)

    @pl.when(core == 1)
    def _():
        with jax.named_scope("join"):
            arrived(joined, c_recv)
        for i in range(2):
            part = pl.ds(i * rank, rank)
            partial[part, :] = (totals[i] + joined[part, :].astype(f32)).astype(bf16)
        for k in range(half - 1):
            target = far_first(k)
            send(
                partial.at[pl.ds(target * piece, piece)],
                received.at[lax.rem(target - chip + half, half) - 1],
                rs_send,
                rs_recv,
                {"fs": 2 * target + 1},
            )
        with jax.named_scope("tpsq"):
            spread_squares()
        with jax.named_scope("rs"):
            arrived(received, rs_recv)
        own = partial[pl.ds(pl.multiple_of(chip * piece, piece), piece), :]
        gathered[chip] = (
            own.astype(f32) + jnp.sum(received[...].astype(f32), axis=0)
        ).astype(bf16)
        for k in range(half - 1):
            send(
                gathered.at[chip],
                gathered.at[chip],
                ag_send,
                ag_recv.at[chip],
                {"fs": 2 * far_first(k) + 1},
            )
        send(gathered.at[chip], gathered.at[chip], p_send, p_recv, {"fs": partner})
        for k in range(half - 1):
            source = near_first(k)
            with jax.named_scope(f"ag{k}"):
                arrived(gathered.at[source], ag_recv.at[source])
            send(
                gathered.at[source],
                gathered.at[source],
                p_send,
                p_recv,
                {"fs": partner},
            )
        with jax.named_scope("xw"):
            arrived(weights.at[partner], x_recv)
        with jax.named_scope("fw"):
            arrived(weights.at[pl.ds(0, n - 2)], f_recv)
        left(received, rs_send)
        left(gathered.at[pl.ds(0, half - 1)], ag_send)
        with jax.named_scope("psend"):
            left(gathered, p_send)

    with jax.named_scope("sq"):
        arrived(squares.at[pl.ds(0, n - 1)], s_recv)
    left(squares.at[pl.ds(0, n - 1)], s_send)
    left(tp_squares.at[pl.ds(0, m - 1)], t_send)
    left(weights.at[me], x_send)
    landed(moment_v, load_sem.at[3])


def update_kernel(n, entries, *refs):
    gathered, weights, squares, weight_v, proj_v, moment_v = refs[:6]
    outs, (small, moment, copied), sems = refs[6:16], refs[16:19], refs[19]
    me = lax.axis_index("fs")
    f32, bf16 = jnp.float32, jnp.bfloat16
    rows, cols = weight_v.shape[1:]
    rank = moment_v.shape[1]

    def store(src, out, sem):
        pltpu.make_async_copy(src, outs[out], sems.at[sem]).start()

    both = gathered[...].astype(f32).reshape(2 * rank, cols)
    normalized = []
    for i in range(2):
        projected = both[i * rank : (i + 1) * rank]
        first_new = FIRST_DECAY * moment_v[2 * i] + (1.0 - FIRST_DECAY) * projected
        second_new = (
            SECOND_DECAY * moment_v[2 * i + 1]
            + (1.0 - SECOND_DECAY) * projected * projected
        )
        moment[2 * i] = first_new
        moment[2 * i + 1] = second_new
        store(moment.at[2 * i], 4 + 2 * i, 1)
        store(moment.at[2 * i + 1], 5 + 2 * i, 1)
        normalized.append((first_new / (jnp.sqrt(second_new) + EPSILON)).astype(bf16))
    tile = jnp.sum(squares[...], axis=0)
    for i in range(2):
        total = jnp.sum(tile[i : i + 1], keepdims=True)
        scale = LEARN_RATE * jnp.sqrt(total / entries)
        every = scale * jnp.dot(proj_v[i], normalized[i], preferred_element_type=f32)
        held = weights[:, i].astype(f32).reshape(n * rows, cols)
        copied[i] = (held - every).astype(bf16)
        store(copied.at[i], 8 + i, 2)
        own = proj_v[i, pl.ds(pl.multiple_of(me * rows, rows), rows), :]
        own_step = scale * jnp.dot(own, normalized[i], preferred_element_type=f32)
        small[2 + i] = own_step
        small[i] = weight_v[i] - own_step
        store(small.at[2 + i], 2 + i, 0)
        store(small.at[i], i, 0)
    for sem, ref in enumerate((small, moment, copied)):
        pltpu.make_async_copy(ref, ref, sems.at[sem]).wait()


def solution(mesh):
    n, m = mesh.shape["fs"], mesh.shape["tp"]

    def body(
        latent,
        key_cot,
        value_cot,
        key_weight,
        value_weight,
        key_proj,
        value_proj,
        key_first,
        key_second,
        value_first,
        value_second,
    ):
        f32, bf16 = jnp.float32, jnp.bfloat16
        sds = jax.ShapeDtypeStruct
        tokens, width = latent.shape
        rows, cols = key_weight.shape
        rank = key_proj.shape[1]
        half = n // 2
        piece = 2 * rank // half
        dma = pltpu.SemaphoreType.DMA
        held = pl.pallas_call(
            functools.partial(exchange_kernel, n, m),
            out_shape=(
                sds((half, piece, cols), bf16),
                sds((n, 2, rows, cols), bf16),
                sds((n, 2, cols), f32),
                sds((2, rows, cols), f32),
                sds((2, width, rank), bf16),
                sds((4, rank, cols), f32),
            ),
            in_specs=[HBM] * 11,
            out_specs=(VMEM,) * 6,
            scratch_shapes=[
                pltpu.VMEM((CHUNKS, tokens, width // CHUNKS), bf16),
                pltpu.VMEM((2, tokens, cols), bf16),
                pltpu.VMEM((2 * cols, tokens), bf16),
                pltpu.VMEM((2 * cols, width), bf16),
                pltpu.VMEM((2 * rank, cols), bf16),
                pltpu.VMEM((2 * rank, cols), bf16),
                pltpu.VMEM((half - 1, piece, cols), bf16),
                pltpu.VMEM((m, 2, cols), f32),
                dma((4,)),
                dma((CHUNKS,)),
                dma,
                dma,
                dma,
                dma,
                dma,
                dma,
                dma,
                dma,
                dma,
                dma((half,)),
                dma,
                dma,
                dma,
                dma,
                dma,
                dma((n,)),
                dma,
                dma,
                dma,
            ],
            compiler_params=pltpu.CompilerParams(
                collective_id=0, has_side_effects=True, vmem_limit_bytes=24 << 20
            ),
        )(
            *(
                pltpu.with_memory_space_constraint(x, pltpu.MemorySpace.HBM)
                for x in (
                    latent,
                    key_cot,
                    value_cot,
                    key_weight,
                    value_weight,
                    key_proj,
                    value_proj,
                    key_first,
                    key_second,
                    value_first,
                    value_second,
                )
            )
        )
        small = sds((rows, cols), f32)
        moment = sds((rank, cols), f32)
        copy = sds((n * rows, cols), bf16)
        return pl.pallas_call(
            functools.partial(update_kernel, n, float(rows * cols * n * m)),
            out_shape=(small,) * 4 + (moment,) * 4 + (copy,) * 2,
            in_specs=[VMEM] * 6,
            out_specs=(HBM,) * 10,
            scratch_shapes=[
                pltpu.VMEM((4, rows, cols), f32),
                pltpu.VMEM((4, rank, cols), f32),
                pltpu.VMEM((2, n * rows, cols), bf16),
                dma((3,)),
            ],
            compiler_params=pltpu.CompilerParams(vmem_limit_bytes=24 << 20),
        )(*held)

    split, column = P("fs", "tp"), P(None, "tp")
    return jax.shard_map(
        body,
        mesh=mesh,
        in_specs=(P("fs", None),) + (split,) * 4 + (P(),) * 2 + (column,) * 4,
        out_specs=(split,) * 4 + (column,) * 6,
        check_vma=False,
    )
```

time: 22.8 us -> 21.5 us (0.943)
  Pallas kernels: 21.9 us -> 20.6 us
    pallas_call x1, Pallas kernels: 20.4 us -> 19.1 us  [body(): pl.pallas_call(functools.partial(exchange_kernel, n, m), out_shape=(sds((...]
where the time goes in v1:
time: 21.5 us; the launch traced here: 21.3 us
  Pallas kernels  20.6 us (96%)
  between operations  0.65 us (3%)
    pallas_call x1, Pallas kernels, body(): pl.pallas_call(functools.partial(exchange_kernel, n, m), out_shape=(sds((...  19.1 us
    pallas_call x1, Pallas kernels, body(): pl.pallas_call(functools.partial(update_kernel, n, float(rows * cols * n...  1.54 us

profile of v1, /device:TPU:0, one launch (start us, length us, event | category | flops | bytes accessed | tf_op | source)
XLA Modules:
  0.0 21.3 jit_solution(2773989197978784629)
XLA Ops:
  0.6 19.1 %shard_map.186 = (bf16[4,128,128]{2,1,0:T(8,128)(2,1)S(1)}, bf16[8,2,128,128]{3,2,1,0:T(8,128)(2,1)S(1)}, f32[8,2,128]{2,1,0:T(2,128)S(1)}, f32[2,128,128]{2,1,0...) custom-call(bf16[2048,1024]{1,0:T(8,128)(2,1)} %latent.1, bf16[2048,128]{1,0:T(8,128)(2,1)} %key_cot.1, ...), custom_call_target="tpu_custom_call" | custom-call | tf_op jit(solution)/shard_map/pallas_call | solution.py:402
  19.8 1.5 %shard_map.187 = (f32[128,128]{1,0:T(8,128)}, f32[128,128]{1,0:T(8,128)}, f32[128,128]{1,0:T(8,128)}, f32[128,128]{1,0:T(8,128)}, f32[256,128]{1,0:T(8,128)}, /*...) custom-call(bf16[4,128,128]{2,1,0:T(8,128)(2,1)S(1)} %get-tuple-elem, ...), custom_call_target="tpu_custom_call" | custom-call | tf_op jit(solution)/shard_map/pallas_call | solution.py:469

commit v2 on v1

v2 whole, which is shorter than its diff:
```python
import functools

import jax
import jax.numpy as jnp
from jax import lax
from jax.experimental import pallas as pl
from jax.experimental.pallas import tpu as pltpu
from jax.sharding import PartitionSpec as P

EPSILON = 1e-08
FIRST_DECAY = 0.7
SECOND_DECAY = 0.8
LEARN_RATE = 0.2
CUTS = (0, 1, 2, 4)
BARRIER_CHUNK = 1
DOT_COLS = 256
MESH = pl.DeviceIdType.MESH
HBM = pl.BlockSpec(memory_space=pltpu.MemorySpace.HBM)
VMEM = pl.BlockSpec(memory_space=pltpu.MemorySpace.VMEM)


def exchange_kernel(
    n,
    m,
    entries,
    latent,
    key_cot,
    value_cot,
    key_weight,
    value_weight,
    key_proj,
    value_proj,
    key_first,
    key_second,
    value_first,
    value_second,
    small,
    moment,
    copied,
    gathered,
    weights,
    weight_v,
    proj_v,
    moment_v,
    latent_v,
    cot_v,
    cot_t,
    reduced,
    partial,
    joined,
    turned,
    steps,
    received,
    own_squares,
    hub_squares,
    tp_squares,
    squares,
    load_sem,
    latent_sem,
    send_sem,
    recv_sem,
    weight_sem,
    square_sem,
):
    me = lax.axis_index("fs")
    mine = lax.axis_index("tp")
    core = lax.rem(me, 2)
    chip = lax.div(me, 2)
    partner = me + 1 - 2 * core
    half = n // 2
    width = latent.shape[1]
    rank = key_proj.shape[1]
    rows, cols = key_weight.shape
    owners, piece = gathered.shape[:2]
    first_owner = (half - owners) // 2
    f32, bf16 = jnp.float32, jnp.bfloat16
    chunks = [
        (a * width // CUTS[-1], (b - a) * width // CUTS[-1])
        for a, b in zip(CUTS, CUTS[1:])
    ]

    def load(src, dst, sem):
        pltpu.make_async_copy(src, dst, sem).start()

    def landed(ref, sem):
        pltpu.make_async_copy(ref, ref, sem).wait()

    load(key_cot, cot_v.at[0], load_sem.at[0])
    load(value_cot, cot_v.at[1], load_sem.at[0])
    for c, (start, size) in enumerate(chunks):
        part = (slice(None), pl.ds(start, size))
        load(latent.at[part], latent_v.at[part], latent_sem.at[c])
        if c == 0:
            load(key_weight, weight_v.at[0], load_sem.at[1])
            load(value_weight, weight_v.at[1], load_sem.at[1])

    barrier = pltpu.get_barrier_semaphore()
    for d in range(1, n):
        pl.semaphore_signal(
            barrier, inc=1, device_id={"fs": lax.rem(me + d, n)}, device_id_type=MESH
        )

    hub = me == 0

    @pl.when(hub)
    def _():
        for d in range(1, m):
            pl.semaphore_signal(
                barrier,
                inc=1,
                device_id={"tp": lax.rem(mine + d, m)},
                device_id_type=MESH,
            )

    def remote(src, dst, sem, arrival, where):
        return pltpu.make_async_remote_copy(
            src_ref=src,
            dst_ref=dst,
            send_sem=sem,
            recv_sem=arrival,
            device_id=where,
            device_id_type=MESH,
        )

    def send(src, dst, arrival, where):
        remote(src, dst, send_sem, arrival, where).start()

    def arrived(ref, sem):
        remote(ref, ref, sem, sem, {"fs": partner}).wait_recv()

    def left(ref, sem):
        remote(ref, ref, sem, sem, {"fs": partner}).wait_send()

    def all_left(elements):
        left(latent_v.at[pl.ds(0, elements // width)], send_sem)

    side = lax.div(chip, (half + 1) // 2)

    def far_first(k):
        down = half - 1 - k
        down = down - lax.div(chip - down + half, half)
        up = k + lax.div(k - chip + half, half)
        return down + side * (up - down)

    def near_first(k):
        return far_first(half - 2 - k)

    def direct(source, target):
        return (
            ((target > 0) & (target < half - 1))
            | (abs(target - source) <= 1)
            | ((target == 0) & (source == 2))
        )

    def late(source, target):
        return (source == 2) & (target == 1)

    def direct_count(c):
        return sum(bool(direct(c, t)) for t in range(half) if t != c)

    def relay_count(c):
        return sum(
            2 * (not direct(t, end))
            for end, near in ((0, 1), (half - 1, half - 2))
            for t in range(half)
            if c == near
        )

    piece_at, weight_at = recv_sem.at[0], recv_sem.at[1]

    def join_at(i):
        return recv_sem.at[3 + owners + i]

    partner_at = recv_sem.at[0]

    def total_at(i):
        return recv_sem.at[1 + i]

    def summed_at(owner):
        return recv_sem.at[3 + owner]

    def owns(c):
        return (c >= first_owner) & (c < first_owner + owners)

    def shard_at(source, i):
        return weight_sem.at[source, i]

    def spread(now_late):
        for i in range(2):
            for k in range(half - 1):
                target = far_first(k)

                @pl.when(direct(chip, target) & (late(chip, target) == now_late))
                def _():
                    send(
                        weights.at[me, i],
                        weights.at[me, i],
                        shard_at(me, i),
                        {"fs": 2 * target},
                    )

    def enter():
        with jax.named_scope("bar"):
            pl.semaphore_wait(barrier, n - 1 + jnp.where(hub, m - 1, 0))

        @pl.when(~hub)
        def _():
            remote(
                own_squares,
                hub_squares.at[me],
                square_sem.at[0],
                square_sem.at[1],
                {"fs": 0},
            ).start()

        spread(False)

        @pl.when(core == 0)
        def _():
            send(weights.at[me], weights.at[me], weight_at, {"fs": partner})

        @pl.when(core == 1)
        def _():
            send(weights.at[me], weights.at[me], partner_at, {"fs": partner})

    with jax.named_scope("cot"):
        landed(cot_v, load_sem.at[0])
    for i in range(2):
        cot_t[pl.ds(i * cols, cols), :] = cot_v[i].T

    for c, (start, size) in enumerate(chunks):
        if c == BARRIER_CHUNK:
            with jax.named_scope("wt"):
                landed(weight_v, load_sem.at[1])
            for i in range(2):
                w = weight_v[i]
                weights[me, i] = w.astype(bf16)
                own_squares[pl.ds(i, 1), :] = jnp.sum(w * w, axis=0, keepdims=True)
            pl.when(chip > 0)(enter)

        part = pl.ds(start, size)
        with jax.named_scope(f"lat{c}"):
            landed(latent_v.at[:, part], latent_sem.at[c])
        if c == 0:
            load(key_proj, proj_v.at[0], load_sem.at[0])
            load(value_proj, proj_v.at[1], load_sem.at[0])
        if c == BARRIER_CHUNK:
            load(key_first, moment_v.at[0], load_sem.at[1])
            load(key_second, moment_v.at[1], load_sem.at[1])
            load(value_first, moment_v.at[2], load_sem.at[1])
            load(value_second, moment_v.at[3], load_sem.at[1])
        for at in range(start, start + size, DOT_COLS):
            for i in range(2):
                head = pl.ds(i * cols, cols)
                reduced[head, pl.ds(at, DOT_COLS)] = jnp.dot(
                    cot_t[head, :],
                    latent_v[:, pl.ds(at, DOT_COLS)],
                    preferred_element_type=f32,
                ).astype(bf16)
    landed(proj_v, load_sem.at[0])
    totals = [
        jnp.dot(
            reduced[pl.ds(i * cols, cols), :], proj_v[i], preferred_element_type=f32
        )
        for i in range(2)
    ]
    pl.when(chip == 0)(enter)

    @pl.when(core == 0)
    def _():
        for i in range(2):
            part = pl.ds(i * rank, rank)
            partial[part, :] = totals[i].astype(bf16).T
            send(partial.at[part], joined.at[part], join_at(i), {"fs": partner})
        shift = jnp.where(chip == 1, 2, jnp.where(chip == half - 2, 1, 0))
        for k in range(half - 1):
            if k == 0:

                @pl.when(hub)
                def _():
                    with jax.named_scope("hub"):
                        arrived(hub_squares.at[pl.ds(1, n - 1)], square_sem.at[1])
                    hub_squares[0] = own_squares[...]
                    tp_squares[mine] = jnp.sum(hub_squares[...], axis=0)
                    for d in range(1, m):
                        remote(
                            tp_squares.at[mine],
                            tp_squares.at[mine],
                            square_sem.at[2],
                            square_sem.at[3],
                            {"tp": lax.rem(mine + d, m)},
                        ).start()

            if k == min(1, half - 2):
                spread(True)

            if k == half - 2:

                @pl.when(hub)
                def _():
                    with jax.named_scope("hubtp"):
                        arrived(tp_squares.at[pl.ds(0, m - 1)], square_sem.at[3])
                    squares[...] = jnp.sum(tp_squares[...], axis=0)
                    for d in range(1, n):
                        remote(
                            squares,
                            squares,
                            square_sem.at[0],
                            square_sem.at[1],
                            {"fs": d},
                        ).start()

            origin = near_first(lax.rem(k + shift, half - 1))
            for i in range(2):
                for part in range(2):
                    source = 2 * origin + part
                    shard = weights.at[source, i]
                    with jax.named_scope(f"w{k}{i}{part}"):
                        arrived(shard, shard_at(source, i))
                    for end, near in ((0, 1), (half - 1, half - 2)):

                        @pl.when((chip == near) & ~direct(origin, end))
                        def _():
                            send(shard, shard, shard_at(source, i), {"fs": 2 * end})

                    send(shard, shard, weight_at, {"fs": partner})
        with jax.named_scope("xw"):
            arrived(weights.at[partner], partner_at)

    @pl.when(core == 1)
    def _():
        for i in range(2):
            turned[i] = totals[i].T
        for i in range(2):
            part = pl.ds(i * rank, rank)
            with jax.named_scope(f"join{i}"):
                arrived(joined.at[part], join_at(i))
            partial[part, :] = (turned[i] + joined[part, :].astype(f32)).astype(bf16)
        for k in range(half - 1):
            target = far_first(lax.rem(k + side, half - 1))

            @pl.when(owns(target))
            def _():
                send(
                    partial.at[pl.ds((target - first_owner) * piece, piece)],
                    received.at[lax.rem(target - chip + half, half) - 1],
                    piece_at,
                    {"fs": 2 * target + 1},
                )

        spread(True)

        @pl.when(owns(chip))
        def _():
            mine_at = chip - first_owner
            with jax.named_scope("rs"):
                arrived(received, piece_at)
            own = partial[pl.ds(pl.multiple_of(mine_at * piece, piece), piece), :]
            gathered[mine_at] = (
                own.astype(f32) + jnp.sum(received[...].astype(f32), axis=0)
            ).astype(bf16)
            for k in range(half - 1):
                send(
                    gathered.at[mine_at],
                    gathered.at[mine_at],
                    summed_at(mine_at),
                    {"fs": 2 * far_first(k) + 1},
                )
            send(
                gathered.at[mine_at],
                gathered.at[mine_at],
                total_at(lax.div(2 * mine_at, owners)),
                {"fs": partner},
            )

        for k in range(half - 1):
            source = near_first(k)

            @pl.when(owns(source))
            def _():
                owner = source - first_owner
                with jax.named_scope(f"ag{k}"):
                    arrived(gathered.at[owner], summed_at(owner))
                send(
                    gathered.at[owner],
                    gathered.at[owner],
                    total_at(lax.div(2 * owner, owners)),
                    {"fs": partner},
                )

    landed(moment_v, load_sem.at[1])

    @pl.when(core == 0)
    def _():
        for i in range(2):
            with jax.named_scope(f"final{i}"):
                arrived(gathered.at[pl.ds(i * owners // 2, owners // 2)], total_at(i))

    both = gathered[...].astype(f32).reshape(2 * rank, cols)
    normalized = []
    for i in range(2):
        projected = both[i * rank : (i + 1) * rank]
        first_new = FIRST_DECAY * moment_v[2 * i] + (1.0 - FIRST_DECAY) * projected
        second_new = (
            SECOND_DECAY * moment_v[2 * i + 1]
            + (1.0 - SECOND_DECAY) * projected * projected
        )
        moment[2 * i] = first_new
        moment[2 * i + 1] = second_new
        normalized.append((first_new / (jnp.sqrt(second_new) + EPSILON)).astype(bf16))

    @pl.when(~hub)
    def _():
        with jax.named_scope("sq"):
            arrived(squares, square_sem.at[1])

    for i in range(2):
        total = jnp.sum(squares[pl.ds(i, 1), :], keepdims=True)
        scale = LEARN_RATE * jnp.sqrt(total / entries)
        steps[i] = scale * jnp.dot(
            proj_v[i], normalized[i], preferred_element_type=f32
        )

    @pl.when(core == 1)
    def _():
        with jax.named_scope("fw"):
            arrived(weights.at[pl.ds(0, n - 1)], weight_at)

    for i in range(2):
        own_step = steps[i, pl.ds(pl.multiple_of(me * rows, rows), rows), :]
        small[2 + i] = own_step
        small[i] = weight_v[i] - own_step
        held = weights[:, i].astype(f32).reshape(n * rows, cols)
        copied[i] = (held - steps[i]).astype(bf16)

    shard_size = 2 * rows * cols
    for c in range(half):
        sent_pieces = 2 * owners
        if first_owner <= c < first_owner + owners:
            sent_pieces += half - 2
        shards = [1 + direct_count(c)] * 2
        shards[0] += n - 2 + relay_count(c)

        @pl.when((chip == c) & (core == 0))
        def _():
            all_left(2 * rank * cols + shards[0] * shard_size)

        @pl.when((chip == c) & (core == 1))
        def _():
            all_left(sent_pieces * piece * cols + shards[1] * shard_size)

    @pl.when(hub)
    def _():
        left(tp_squares.at[pl.ds(0, m - 1)], square_sem.at[2])
        left(hub_squares.at[pl.ds(0, n - 1)], square_sem.at[0])

    @pl.when(~hub)
    def _():
        left(own_squares, square_sem.at[0])


def store_kernel(small, moment, copied, *refs):
    outs, sems = refs[:10], refs[10]
    pairs = [(moment.at[i], outs[4 + i], 0) for i in range(4)]
    pairs += [(copied.at[i], outs[8 + i], 1) for i in range(2)]
    pairs += [(small.at[i], outs[i], 2) for i in range(4)]
    for src, out, sem in pairs:
        pltpu.make_async_copy(src, out, sems.at[sem]).start()
    for sem, ref in enumerate((moment, copied, small)):
        pltpu.make_async_copy(ref, ref, sems.at[sem]).wait()


def solution(mesh):
    n, m = mesh.shape["fs"], mesh.shape["tp"]
    half = n // 2
    owners = half

    def body(latent, key_cot, value_cot, key_weight, value_weight, key_proj, *rest):
        f32, bf16 = jnp.float32, jnp.bfloat16
        sds = jax.ShapeDtypeStruct
        tokens, width = latent.shape
        rows, cols = key_weight.shape
        rank = key_proj.shape[1]
        piece = 2 * rank // owners
        dma = pltpu.SemaphoreType.DMA
        operands = latent, key_cot, value_cot, key_weight, value_weight, key_proj, *rest
        held = pl.pallas_call(
            functools.partial(exchange_kernel, n, m, float(rows * cols * n * m)),
            out_shape=(
                sds((4, rows, cols), f32),
                sds((4, rank, cols), f32),
                sds((2, n * rows, cols), bf16),
            ),
            in_specs=[HBM] * 11,
            out_specs=(VMEM,) * 3,
            scratch_shapes=[
                pltpu.VMEM((owners, piece, cols), bf16),
                pltpu.VMEM((n, 2, rows, cols), bf16),
                pltpu.VMEM((2, rows, cols), f32),
                pltpu.VMEM((2, width, rank), bf16),
                pltpu.VMEM((4, rank, cols), f32),
                pltpu.VMEM((tokens, width), bf16),
                pltpu.VMEM((2, tokens, cols), bf16),
                pltpu.VMEM((2 * cols, tokens), bf16),
                pltpu.VMEM((2 * cols, width), bf16),
                pltpu.VMEM((2 * rank, cols), bf16),
                pltpu.VMEM((2 * rank, cols), bf16),
                pltpu.VMEM((2, rank, cols), f32),
                pltpu.VMEM((2, n * rows, cols), f32),
                pltpu.VMEM((half - 1, piece, cols), bf16),
                pltpu.VMEM((2, cols), f32),
                pltpu.VMEM((n, 2, cols), f32),
                pltpu.VMEM((m, 2, cols), f32),
                pltpu.VMEM((2, cols), f32),
                dma((2,)),
                dma((len(CUTS) - 1,)),
                dma,
                dma((5 + owners,)),
                dma((n, 2)),
                dma((4,)),
            ],
            compiler_params=pltpu.CompilerParams(
                collective_id=0, has_side_effects=True, vmem_limit_bytes=24 << 20
            ),
        )(
            *(
                pltpu.with_memory_space_constraint(x, pltpu.MemorySpace.HBM)
                for x in operands
            )
        )
        return pl.pallas_call(
            store_kernel,
            out_shape=(sds((rows, cols), f32),) * 4
            + (sds((rank, cols), f32),) * 4
            + (sds((n * rows, cols), bf16),) * 2,
            in_specs=[VMEM] * 3,
            out_specs=(HBM,) * 10,
            scratch_shapes=[dma((3,))],
            compiler_params=pltpu.CompilerParams(vmem_limit_bytes=24 << 20),
        )(*held)

    split, column = P("fs", "tp"), P(None, "tp")
    return jax.shard_map(
        body,
        mesh=mesh,
        in_specs=(P("fs", None),) + (split,) * 4 + (P(),) * 2 + (column,) * 4,
        out_specs=(split,) * 4 + (column,) * 6,
        check_vma=False,
    )
```

time: 21.5 us -> 17.8 us (0.83)
  Pallas kernels: 20.6 us -> 17 us
    pallas_call x2, Pallas kernels: 20.6 us -> 17 us  [the longest x1 15.9 us: body(): pl.pallas_call(functools.partial(exchange_kernel, n, m, float(rows * cols...]
where the time goes in v2:
time: 17.8 us; the launch traced here: 17.6 us
  Pallas kernels  17 us (96%)
  between operations  0.65 us (4%)
    pallas_call x1, Pallas kernels, body(): pl.pallas_call(functools.partial(exchange_kernel, n, m, float(rows * cols...  15.9 us
    pallas_call x1, Pallas kernels, body(): pl.pallas_call(store_kernel, out_shape=(sds((rows, cols), f32),) * 4 + (s...  1.07 us

profile of v2, /device:TPU:0, one launch (start us, length us, event | category | flops | bytes accessed | tf_op | source)
XLA Modules:
  0.0 17.6 jit_solution(12203930924113961441)
XLA Ops:
  0.6 15.9 %shard_map.186 = (f32[4,128,128]{2,1,0:T(8,128)S(1)}, f32[4,256,128]{2,1,0:T(8,128)S(1)}, bf16[2,1024,128]{2,1,0:T(8,128)(2,1)S(1)}) custom-call(bf16[2048,1024]{1,0:T(8,128)(2,1)} %latent.1, bf16[2048,128]{1,0:T(8,128)(2,1)} %key_cot.1, bf16[2048,128]{1,0:T(8,128)(2,1)} %value_cot.1, f32[128,128]{1,0:T(8,128)} %key_weight.1, f32[128,128]{1,0:T(8,128)} %value_weight.1, ...), custom_call_target="tpu_custom_call" | custom-call | tf_op jit(solution)/shard_map/pallas_call | solution.py:487
  16.6 1.1 %shard_map.187 = (f32[128,128]{1,0:T(8,128)}, f32[128,128]{1,0:T(8,128)}, f32[128,128]{1,0:T(8,128)}, f32[128,128]{1,0:T(8,128)}, f32[256,128]{1,0:T(8,128)}, /*...) custom-call(f32[4,128,128]{2,1,0:T(8,128)S(1)} %get-tuple-element.13, ...), custom_call_target="tpu_custom_call" | custom-call | tf_op jit(solution)/shard_map/pallas_call | solution.py:531

commit v3 on v2

--- a/solution.py
+++ b/solution.py
@@ -50,6 +50,7 @@
     joined,
     turned,
     steps,
+    normalized,
     received,
     own_squares,
     hub_squares,
@@ -59,7 +60,6 @@
     latent_sem,
     send_sem,
     recv_sem,
-    weight_sem,
     square_sem,
 ):
     me = lax.axis_index("fs")
@@ -71,8 +71,7 @@
     width = latent.shape[1]
     rank = key_proj.shape[1]
     rows, cols = key_weight.shape
-    owners, piece = gathered.shape[:2]
-    first_owner = (half - owners) // 2
+    piece = gathered.shape[1]
     f32, bf16 = jnp.float32, jnp.bfloat16
     chunks = [
         (a * width // CUTS[-1], (b - a) * width // CUTS[-1])
@@ -152,8 +151,11 @@
             | ((target == 0) & (source == 2))
         )
 
-    def late(source, target):
-        return (source == 2) & (target == 1)
+    def turn(target):
+        last = ((chip == 2) & (target == 1)) | (
+            (chip == half - 1) & (target == half - 2)
+        )
+        return jnp.where(last, 2, jnp.where((core == 1) & (chip == 0), 1, 0))
 
     def direct_count(c):
         return sum(bool(direct(c, t)) for t in range(half) if t != c)
@@ -166,36 +168,36 @@
             if c == near
         )
 
+    def slot(source, target):
+        return lax.rem(source - target + half, half) - 1
+
     piece_at, weight_at = recv_sem.at[0], recv_sem.at[1]
 
     def join_at(i):
-        return recv_sem.at[3 + owners + i]
+        return recv_sem.at[2 + i]
+
+    def summed_at(owner, target):
+        return recv_sem.at[4 + slot(owner, target)]
 
     partner_at = recv_sem.at[0]
 
-    def total_at(i):
-        return recv_sem.at[1 + i]
-
-    def summed_at(owner):
-        return recv_sem.at[3 + owner]
-
-    def owns(c):
-        return (c >= first_owner) & (c < first_owner + owners)
-
-    def shard_at(source, i):
-        return weight_sem.at[source, i]
-
-    def spread(now_late):
+    def total_at(owner):
+        return recv_sem.at[1 + owner]
+
+    def shard_at(source, target, i):
+        return recv_sem.at[1 + half + 2 * slot(source, target) + i]
+
+    def spread(now):
         for i in range(2):
             for k in range(half - 1):
                 target = far_first(k)
 
-                @pl.when(direct(chip, target) & (late(chip, target) == now_late))
+                @pl.when(direct(chip, target) & (turn(target) == now))
                 def _():
                     send(
                         weights.at[me, i],
                         weights.at[me, i],
-                        shard_at(me, i),
+                        shard_at(chip, target, i),
                         {"fs": 2 * target},
                     )
 
@@ -213,7 +215,7 @@
                 {"fs": 0},
             ).start()
 
-        spread(False)
+        spread(0)
 
         @pl.when(core == 0)
         def _():
@@ -292,7 +294,7 @@
                         ).start()
 
             if k == min(1, half - 2):
-                spread(True)
+                spread(2)
 
             if k == half - 2:
 
@@ -312,18 +314,18 @@
 
             origin = near_first(lax.rem(k + shift, half - 1))
             for i in range(2):
-                for part in range(2):
-                    source = 2 * origin + part
-                    shard = weights.at[source, i]
-                    with jax.named_scope(f"w{k}{i}{part}"):
-                        arrived(shard, shard_at(source, i))
-                    for end, near in ((0, 1), (half - 1, half - 2)):
-
-                        @pl.when((chip == near) & ~direct(origin, end))
-                        def _():
-                            send(shard, shard, shard_at(source, i), {"fs": 2 * end})
-
-                    send(shard, shard, weight_at, {"fs": partner})
+                shards = weights.at[pl.ds(2 * origin, 2), i]
+                with jax.named_scope(f"w{k}{i}"):
+                    arrived(shards, shard_at(origin, chip, i))
+                for end, near in ((0, 1), (half - 1, half - 2)):
+
+                    @pl.when((chip == near) & ~direct(origin, end))
+                    def _():
+                        send(
+                            shards, shards, shard_at(origin, end, i), {"fs": 2 * end}
+                        )
+
+                send(shards, shards, weight_at, {"fs": partner})
         with jax.named_scope("xw"):
             arrived(weights.at[partner], partner_at)
 
@@ -338,88 +340,77 @@
             partial[part, :] = (turned[i] + joined[part, :].astype(f32)).astype(bf16)
         for k in range(half - 1):
             target = far_first(lax.rem(k + side, half - 1))
-
-            @pl.when(owns(target))
+            send(
+                partial.at[pl.ds(target * piece, piece)],
+                received.at[slot(chip, target)],
+                piece_at,
+                {"fs": 2 * target + 1},
+            )
+        spread(1)
+        with jax.named_scope("rs"):
+            arrived(received, piece_at)
+        own = partial[pl.ds(pl.multiple_of(chip * piece, piece), piece), :]
+        gathered[chip] = (
+            own.astype(f32) + jnp.sum(received[...].astype(f32), axis=0)
+        ).astype(bf16)
+        for k in range(half - 1):
+            target = far_first(k)
+            send(
+                gathered.at[chip],
+                gathered.at[chip],
+                summed_at(chip, target),
+                {"fs": 2 * target + 1},
+            )
+        send(gathered.at[chip], gathered.at[chip], total_at(chip), {"fs": partner})
+        spread(2)
+        for k in range(half - 1):
+            owner = near_first(k)
+            with jax.named_scope(f"ag{k}"):
+                arrived(gathered.at[owner], summed_at(owner, chip))
+            send(
+                gathered.at[owner], gathered.at[owner], total_at(owner), {"fs": partner}
+            )
+
+    landed(moment_v, load_sem.at[1])
+
+    for owner in range(half):
+
+        @pl.when(core == 0)
+        def _():
+            with jax.named_scope(f"final{owner}"):
+                arrived(gathered.at[owner], total_at(owner))
+
+        i, start = divmod(owner * piece, rank)
+        part = pl.ds(start, piece)
+        projected = gathered[owner].astype(f32)
+        first_new = (
+            FIRST_DECAY * moment_v[2 * i, part, :] + (1.0 - FIRST_DECAY) * projected
+        )
+        second_new = (
+            SECOND_DECAY * moment_v[2 * i + 1, part, :]
+            + (1.0 - SECOND_DECAY) * projected * projected
+        )
+        moment[2 * i, part, :] = first_new
+        moment[2 * i + 1, part, :] = second_new
+        normalized[i, part, :] = (
+            first_new / (jnp.sqrt(second_new) + EPSILON)
+        ).astype(bf16)
+        if start + piece < rank:
+            continue
+        if i == 0:
+
+            @pl.when(~hub)
             def _():
-                send(
-                    partial.at[pl.ds((target - first_owner) * piece, piece)],
-                    received.at[lax.rem(target - chip + half, half) - 1],
-                    piece_at,
-                    {"fs": 2 * target + 1},
-                )
-
-        spread(True)
-
-        @pl.when(owns(chip))
-        def _():
-            mine_at = chip - first_owner
-            with jax.named_scope("rs"):
-                arrived(received, piece_at)
-            own = partial[pl.ds(pl.multiple_of(mine_at * piece, piece), piece), :]
-            gathered[mine_at] = (
-                own.astype(f32) + jnp.sum(received[...].astype(f32), axis=0)
-            ).astype(bf16)
-            for k in range(half - 1):
-                send(
-                    gathered.at[mine_at],
-                    gathered.at[mine_at],
-                    summed_at(mine_at),
-                    {"fs": 2 * far_first(k) + 1},
-                )
-            send(
-                gathered.at[mine_at],
-                gathered.at[mine_at],
-                total_at(lax.div(2 * mine_at, owners)),
-                {"fs": partner},
-            )
-
-        for k in range(half - 1):
-            source = near_first(k)
-
-            @pl.when(owns(source))
-            def _():
-                owner = source - first_owner
-                with jax.named_scope(f"ag{k}"):
-                    arrived(gathered.at[owner], summed_at(owner))
-                send(
-                    gathered.at[owner],
-                    gathered.at[owner],
-                    total_at(lax.div(2 * owner, owners)),
-                    {"fs": partner},
-                )
-
-    landed(moment_v, load_sem.at[1])
-
-    @pl.when(core == 0)
-    def _():
-        for i in range(2):
-            with jax.named_scope(f"final{i}"):
-                arrived(gathered.at[pl.ds(i * owners // 2, owners // 2)], total_at(i))
-
-    both = gathered[...].astype(f32).reshape(2 * rank, cols)
-    normalized = []
-    for i in range(2):
-        projected = both[i * rank : (i + 1) * rank]
-        first_new = FIRST_DECAY * moment_v[2 * i] + (1.0 - FIRST_DECAY) * projected
-        second_new = (
-            SECOND_DECAY * moment_v[2 * i + 1]
-            + (1.0 - SECOND_DECAY) * projected * projected
-        )
-        moment[2 * i] = first_new
-        moment[2 * i + 1] = second_new
-        normalized.append((first_new / (jnp.sqrt(second_new) + EPSILON)).astype(bf16))
-
-    @pl.when(~hub)
-    def _():
-        with jax.named_scope("sq"):
-            arrived(squares, square_sem.at[1])
-
-    for i in range(2):
+                with jax.named_scope("sq"):
+                    arrived(squares, square_sem.at[1])
+
         total = jnp.sum(squares[pl.ds(i, 1), :], keepdims=True)
         scale = LEARN_RATE * jnp.sqrt(total / entries)
-        steps[i] = scale * jnp.dot(
-            proj_v[i], normalized[i], preferred_element_type=f32
-        )
+        for at in range(0, width, width // 2):
+            some = pl.ds(at, width // 2)
+            steps[i, some, :] = scale * jnp.dot(
+                proj_v[i, some, :], normalized[i], preferred_element_type=f32
+            )
 
     @pl.when(core == 1)
     def _():
@@ -435,9 +426,7 @@
 
     shard_size = 2 * rows * cols
     for c in range(half):
-        sent_pieces = 2 * owners
-        if first_owner <= c < first_owner + owners:
-            sent_pieces += half - 2
+        sent_pieces = 3 * half - 2
         shards = [1 + direct_count(c)] * 2
         shards[0] += n - 2 + relay_count(c)
 
@@ -473,7 +462,6 @@
 def solution(mesh):
     n, m = mesh.shape["fs"], mesh.shape["tp"]
     half = n // 2
-    owners = half
 
     def body(latent, key_cot, value_cot, key_weight, value_weight, key_proj, *rest):
         f32, bf16 = jnp.float32, jnp.bfloat16
@@ -481,7 +469,7 @@
         tokens, width = latent.shape
         rows, cols = key_weight.shape
         rank = key_proj.shape[1]
-        piece = 2 * rank // owners
+        piece = 2 * rank // half
         dma = pltpu.SemaphoreType.DMA
         operands = latent, key_cot, value_cot, key_weight, value_weight, key_proj, *rest
         held = pl.pallas_call(
@@ -494,7 +482,7 @@
             in_specs=[HBM] * 11,
             out_specs=(VMEM,) * 3,
             scratch_shapes=[
-                pltpu.VMEM((owners, piece, cols), bf16),
+                pltpu.VMEM((half, piece, cols), bf16),
                 pltpu.VMEM((n, 2, rows, cols), bf16),
                 pltpu.VMEM((2, rows, cols), f32),
                 pltpu.VMEM((2, width, rank), bf16),
@@ -507,6 +495,7 @@
                 pltpu.VMEM((2 * rank, cols), bf16),
                 pltpu.VMEM((2, rank, cols), f32),
                 pltpu.VMEM((2, n * rows, cols), f32),
+                pltpu.VMEM((2, rank, cols), bf16),
                 pltpu.VMEM((half - 1, piece, cols), bf16),
                 pltpu.VMEM((2, cols), f32),
                 pltpu.VMEM((n, 2, cols), f32),
@@ -515,8 +504,7 @@
                 dma((2,)),
                 dma((len(CUTS) - 1,)),
                 dma,
-                dma((5 + owners,)),
-                dma((n, 2)),
+                dma((3 * half - 1,)),
                 dma((4,)),
             ],
             compiler_params=pltpu.CompilerParams(

time: 17.8 us -> 17.6 us (0.989)
  Pallas kernels: 17 us -> 16.8 us
    pallas_call x1, Pallas kernels: 15.9 us -> 15.7 us  [body(): pl.pallas_call(functools.partial(exchange_kernel, n, m, float(rows * cols...]
where the time goes in v3:
time: 17.6 us; the launch traced here: 17.4 us
  Pallas kernels  16.8 us (95%)
  between operations  0.65 us (4%)
    pallas_call x1, Pallas kernels, body(): pl.pallas_call(functools.partial(exchange_kernel, n, m, float(rows * cols...  15.7 us
    pallas_call x1, Pallas kernels, body(): pl.pallas_call(store_kernel, out_shape=(sds((rows, cols), f32),) * 4 + (s...  1.07 us

profile of v3, /device:TPU:0, one launch (start us, length us, event | category | flops | bytes accessed | tf_op | source)
XLA Modules:
  0.0 17.4 jit_solution(14122943683349892506)
XLA Ops:
  0.6 15.7 %shard_map.186 = (f32[4,128,128]{2,1,0:T(8,128)S(1)}, f32[4,256,128]{2,1,0:T(8,128)S(1)}, bf16[2,1024,128]{2,1,0:T(8,128)(2,1)S(1)}) custom-call(bf16[2048,1024]{1,0:T(8,128)(2,1)} %latent.1, bf16[2048,128]{1,0:T(8,128)(2,1)} %key_cot.1, bf16[2048,128]{1,0:T(8,128)(2,1)} %value_cot.1, f32[128,128]{1,0:T(8,128)} %key_weight.1, f32[128,128]{1,0:T(8,128)} %value_weight.1, ...), custom_call_target="tpu_custom_call" | custom-call | tf_op jit(solution)/shard_map/pallas_call | solution.py:475
  16.3 1.1 %shard_map.187 = (f32[128,128]{1,0:T(8,128)}, f32[128,128]{1,0:T(8,128)}, f32[128,128]{1,0:T(8,128)}, f32[128,128]{1,0:T(8,128)}, f32[256,128]{1,0:T(8,128)}, /*...) custom-call(f32[4,128,128]{2,1,0:T(8,128)S(1)} %get-tuple-element.13, ...), custom_call_target="tpu_custom_call" | custom-call | tf_op jit(solution)/shard_map/pallas_call | solution.py:519

commit v4 on v3

--- a/solution.py
+++ b/solution.py
@@ -131,7 +131,12 @@
         remote(ref, ref, sem, sem, {"fs": partner}).wait_send()
 
     def all_left(elements):
-        left(latent_v.at[pl.ds(0, elements // width)], send_sem)
+        across = next(
+            w
+            for w in (width, width // 2, width // 4, width // 8)
+            if elements % (16 * w) == 0 and elements <= w * latent_v.shape[0]
+        )
+        left(latent_v.at[pl.ds(0, elements // across), pl.ds(0, across)], send_sem)
 
     side = lax.div(chip, (half + 1) // 2)
 
@@ -238,7 +243,9 @@
                 w = weight_v[i]
                 weights[me, i] = w.astype(bf16)
                 own_squares[pl.ds(i, 1), :] = jnp.sum(w * w, axis=0, keepdims=True)
-            pl.when(chip > 0)(enter)
+            pl.when(chip > 1)(enter)
+        if c == BARRIER_CHUNK + 1:
+            pl.when(chip == 1)(enter)
 
         part = pl.ds(start, size)
         with jax.named_scope(f"lat{c}"):
@@ -353,8 +360,14 @@
         gathered[chip] = (
             own.astype(f32) + jnp.sum(received[...].astype(f32), axis=0)
         ).astype(bf16)
+        if half > 2:
+
+            @pl.when(chip == 2)
+            def _():
+                send(gathered.at[chip], gathered.at[chip], total_at(chip), {"fs": 0})
+
         for k in range(half - 1):
-            target = far_first(k)
+            target = far_first(jnp.where(chip == 0, half - 2 - k, k))
             send(
                 gathered.at[chip],
                 gathered.at[chip],
@@ -364,14 +377,37 @@
         send(gathered.at[chip], gathered.at[chip], total_at(chip), {"fs": partner})
         spread(2)
         for k in range(half - 1):
-            owner = near_first(k)
-            with jax.named_scope(f"ag{k}"):
-                arrived(gathered.at[owner], summed_at(owner, chip))
-            send(
-                gathered.at[owner], gathered.at[owner], total_at(owner), {"fs": partner}
-            )
+            at_zero = 0 if k == 0 else half - 1 - k
+            at_one = (k + 1) % (half - 1)
+            place = jnp.where(chip == 0, at_zero, jnp.where(chip == 1, at_one, k))
+            owner = near_first(place)
+
+            def take(owner=owner, k=k):
+                with jax.named_scope(f"ag{k}"):
+                    arrived(gathered.at[owner], summed_at(owner, chip))
+
+            if k == half - 2 and half > 2:
+                pl.when(chip > 0)(take)
+            else:
+                take()
+
+            @pl.when((chip > 0) | (owner != 2))
+            def _():
+                send(
+                    gathered.at[owner],
+                    gathered.at[owner],
+                    total_at(owner),
+                    {"fs": partner},
+                )
 
     landed(moment_v, load_sem.at[1])
+
+    def finish(i):
+        own_step = steps[i, pl.ds(pl.multiple_of(me * rows, rows), rows), :]
+        small[2 + i] = own_step
+        small[i] = weight_v[i] - own_step
+        held = weights[:, i].astype(f32).reshape(n * rows, cols)
+        copied[i] = (held - steps[i]).astype(bf16)
 
     for owner in range(half):
 
@@ -379,6 +415,13 @@
         def _():
             with jax.named_scope(f"final{owner}"):
                 arrived(gathered.at[owner], total_at(owner))
+
+        if owner == 2:
+
+            @pl.when((core == 1) & (chip == 0))
+            def _():
+                with jax.named_scope("aglast"):
+                    arrived(gathered.at[2], summed_at(2, 0))
 
         i, start = divmod(owner * piece, rank)
         part = pl.ds(start, piece)
@@ -412,21 +455,20 @@
                 proj_v[i, some, :], normalized[i], preferred_element_type=f32
             )
 
+        pl.when(core == 0)(lambda: finish(i))
+
     @pl.when(core == 1)
     def _():
         with jax.named_scope("fw"):
             arrived(weights.at[pl.ds(0, n - 1)], weight_at)
-
-    for i in range(2):
-        own_step = steps[i, pl.ds(pl.multiple_of(me * rows, rows), rows), :]
-        small[2 + i] = own_step
-        small[i] = weight_v[i] - own_step
-        held = weights[:, i].astype(f32).reshape(n * rows, cols)
-        copied[i] = (held - steps[i]).astype(bf16)
+        for i in range(2):
+            finish(i)
 
     shard_size = 2 * rows * cols
     for c in range(half):
         sent_pieces = 3 * half - 2
+        if half > 2:
+            sent_pieces += (c == 2) - (c == 0)
         shards = [1 + direct_count(c)] * 2
         shards[0] += n - 2 + relay_count(c)
 

time: 17.6 us -> 17.2 us (0.977)
  Pallas kernels: 16.8 us -> 16.2 us
    pallas_call x1, Pallas kernels: 15.7 us -> 15.2 us  [body(): pl.pallas_call(functools.partial(exchange_kernel, n, m, float(rows * cols...]
where the time goes in v4:
time: 17.2 us; the launch traced here: 16.9 us
  Pallas kernels  16.2 us (94%)
  between operations  0.65 us (4%)
    pallas_call x1, Pallas kernels, body(): pl.pallas_call(functools.partial(exchange_kernel, n, m, float(rows * cols...  15.2 us
    pallas_call x1, Pallas kernels, body(): pl.pallas_call(store_kernel, out_shape=(sds((rows, cols), f32),) * 4 + (s...  1.07 us

profile of v4, /device:TPU:0, one launch (start us, length us, event | category | flops | bytes accessed | tf_op | source)
XLA Modules:
  0.0 16.9 jit_solution(1069648860909505318)
XLA Ops:
  0.6 15.2 %shard_map.186 = (f32[4,128,128]{2,1,0:T(8,128)S(1)}, f32[4,256,128]{2,1,0:T(8,128)S(1)}, bf16[2,1024,128]{2,1,0:T(8,128)(2,1)S(1)}) custom-call(bf16[2048,1024]{1,0:T(8,128)(2,1)} %latent.1, bf16[2048,128]{1,0:T(8,128)(2,1)} %key_cot.1, bf16[2048,128]{1,0:T(8,128)(2,1)} %value_cot.1, f32[128,128]{1,0:T(8,128)} %key_weight.1, f32[128,128]{1,0:T(8,128)} %value_weight.1, ...), custom_call_target="tpu_custom_call" | custom-call | tf_op jit(solution)/shard_map/pallas_call | solution.py:517
  15.8 1.1 %shard_map.187 = (f32[128,128]{1,0:T(8,128)}, f32[128,128]{1,0:T(8,128)}, f32[128,128]{1,0:T(8,128)}, f32[128,128]{1,0:T(8,128)}, f32[256,128]{1,0:T(8,128)}, /*...) custom-call(f32[4,128,128]{2,1,0:T(8,128)S(1)} %get-tuple-element.13, ...), custom_call_target="tpu_custom_call" | custom-call | tf_op jit(solution)/shard_map/pallas_call | solution.py:561

commit v5 on v4

--- a/solution.py
+++ b/solution.py
@@ -56,6 +56,7 @@
     hub_squares,
     tp_squares,
     squares,
+    scales,
     load_sem,
     latent_sem,
     send_sem,
@@ -160,7 +161,8 @@
         last = ((chip == 2) & (target == 1)) | (
             (chip == half - 1) & (target == half - 2)
         )
-        return jnp.where(last, 2, jnp.where((core == 1) & (chip == 0), 1, 0))
+        soon = (core == 1) & ((chip == 0) | ((chip == 2) & (target == 1)))
+        return jnp.where(soon, 1, jnp.where(last, 2, 0))
 
     def direct_count(c):
         return sum(bool(direct(c, t)) for t in range(half) if t != c)
@@ -275,6 +277,19 @@
     ]
     pl.when(chip == 0)(enter)
 
+    def set_scales():
+        total = jnp.sum(squares[...], axis=1, keepdims=True)
+        scales[...] = jnp.broadcast_to(
+            LEARN_RATE * jnp.sqrt(total / entries), scales.shape
+        )
+
+    def squares_in():
+        with jax.named_scope("sq"):
+            arrived(squares, square_sem.at[1])
+        set_scales()
+
+    tail = jnp.where(chip == 0, half // 2, 0)
+
     @pl.when(core == 0)
     def _():
         for i in range(2):
@@ -318,6 +333,7 @@
                             square_sem.at[1],
                             {"fs": d},
                         ).start()
+                    set_scales()
 
             origin = near_first(lax.rem(k + shift, half - 1))
             for i in range(2):
@@ -345,14 +361,19 @@
             with jax.named_scope(f"join{i}"):
                 arrived(joined.at[part], join_at(i))
             partial[part, :] = (turned[i] + joined[part, :].astype(f32)).astype(bf16)
-        for k in range(half - 1):
-            target = far_first(lax.rem(k + side, half - 1))
-            send(
-                partial.at[pl.ds(target * piece, piece)],
-                received.at[slot(chip, target)],
-                piece_at,
-                {"fs": 2 * target + 1},
-            )
+            for k in range(half - 1):
+                target = far_first(lax.rem(k + side, half - 1))
+                held_by = jnp.where(target == 0, 1, lax.div(target * piece, rank))
+
+                @pl.when(held_by == i)
+                def _():
+                    send(
+                        partial.at[pl.ds(target * piece, piece)],
+                        received.at[slot(chip, target)],
+                        piece_at,
+                        {"fs": 2 * target + 1},
+                    )
+
         spread(1)
         with jax.named_scope("rs"):
             arrived(received, piece_at)
@@ -360,11 +381,9 @@
         gathered[chip] = (
             own.astype(f32) + jnp.sum(received[...].astype(f32), axis=0)
         ).astype(bf16)
-        if half > 2:
-
-            @pl.when(chip == 2)
-            def _():
-                send(gathered.at[chip], gathered.at[chip], total_at(chip), {"fs": 0})
+        @pl.when(chip == half // 2)
+        def _():
+            send(gathered.at[chip], gathered.at[chip], total_at(chip), {"fs": 0})
 
         for k in range(half - 1):
             target = far_first(jnp.where(chip == 0, half - 2 - k, k))
@@ -377,22 +396,12 @@
         send(gathered.at[chip], gathered.at[chip], total_at(chip), {"fs": partner})
         spread(2)
         for k in range(half - 1):
-            at_zero = 0 if k == 0 else half - 1 - k
-            at_one = (k + 1) % (half - 1)
-            place = jnp.where(chip == 0, at_zero, jnp.where(chip == 1, at_one, k))
-            owner = near_first(place)
-
-            def take(owner=owner, k=k):
+            owner = near_first(jnp.where(chip == 1, (k + 1) % (half - 1), k))
+
+            @pl.when(owner != tail)
+            def _():
                 with jax.named_scope(f"ag{k}"):
                     arrived(gathered.at[owner], summed_at(owner, chip))
-
-            if k == half - 2 and half > 2:
-                pl.when(chip > 0)(take)
-            else:
-                take()
-
-            @pl.when((chip > 0) | (owner != 2))
-            def _():
                 send(
                     gathered.at[owner],
                     gathered.at[owner],
@@ -403,72 +412,83 @@
     landed(moment_v, load_sem.at[1])
 
     def finish(i):
-        own_step = steps[i, pl.ds(pl.multiple_of(me * rows, rows), rows), :]
+        scale = scales[pl.ds(i, 1), :]
+        own_rows = pl.ds(pl.multiple_of(me * rows, rows), rows)
+        own_step = scale * steps[i, own_rows, :]
         small[2 + i] = own_step
         small[i] = weight_v[i] - own_step
         held = weights[:, i].astype(f32).reshape(n * rows, cols)
-        copied[i] = (held - steps[i]).astype(bf16)
-
-    for owner in range(half):
+        copied[i] = (held - scale * steps[i]).astype(bf16)
+
+    second = jnp.where(chip == 0, 1, 0)
+    here = half // 2
+    for turn_of in range(2):
+        i = second if turn_of == 1 else 1 - second
+        for o in range(here) if turn_of == 0 else reversed(range(here)):
+            owner = i * here + o
+
+            @pl.when(core == 0)
+            def _():
+                with jax.named_scope(f"final{turn_of}{o}"):
+                    arrived(gathered.at[owner], total_at(owner))
+
+            if turn_of == 1 and o == 0:
+
+                @pl.when(core == 1)
+                def _():
+                    with jax.named_scope("aglast"):
+                        arrived(gathered.at[tail], summed_at(tail, chip))
+
+                    @pl.when(chip > 0)
+                    def _():
+                        send(
+                            gathered.at[tail],
+                            gathered.at[tail],
+                            total_at(tail),
+                            {"fs": partner},
+                        )
+
+            part = pl.ds(o * piece, piece)
+            projected = gathered[owner].astype(f32)
+            first_new = (
+                FIRST_DECAY * moment_v[2 * i, part, :] + (1.0 - FIRST_DECAY) * projected
+            )
+            second_new = (
+                SECOND_DECAY * moment_v[2 * i + 1, part, :]
+                + (1.0 - SECOND_DECAY) * projected * projected
+            )
+            moment[2 * i, part, :] = first_new
+            moment[2 * i + 1, part, :] = second_new
+            normalized[i, part, :] = (
+                first_new / (jnp.sqrt(second_new) + EPSILON)
+            ).astype(bf16)
+
+        for at in range(0, width, width // 2):
+            some = pl.ds(at, width // 2)
+            steps[i, some, :] = jnp.dot(
+                proj_v[i, some, :], normalized[i], preferred_element_type=f32
+            )
 
         @pl.when(core == 0)
         def _():
-            with jax.named_scope(f"final{owner}"):
-                arrived(gathered.at[owner], total_at(owner))
-
-        if owner == 2:
-
-            @pl.when((core == 1) & (chip == 0))
-            def _():
-                with jax.named_scope("aglast"):
-                    arrived(gathered.at[2], summed_at(2, 0))
-
-        i, start = divmod(owner * piece, rank)
-        part = pl.ds(start, piece)
-        projected = gathered[owner].astype(f32)
-        first_new = (
-            FIRST_DECAY * moment_v[2 * i, part, :] + (1.0 - FIRST_DECAY) * projected
-        )
-        second_new = (
-            SECOND_DECAY * moment_v[2 * i + 1, part, :]
-            + (1.0 - SECOND_DECAY) * projected * projected
-        )
-        moment[2 * i, part, :] = first_new
-        moment[2 * i + 1, part, :] = second_new
-        normalized[i, part, :] = (
-            first_new / (jnp.sqrt(second_new) + EPSILON)
-        ).astype(bf16)
-        if start + piece < rank:
-            continue
-        if i == 0:
-
-            @pl.when(~hub)
-            def _():
-                with jax.named_scope("sq"):
-                    arrived(squares, square_sem.at[1])
-
-        total = jnp.sum(squares[pl.ds(i, 1), :], keepdims=True)
-        scale = LEARN_RATE * jnp.sqrt(total / entries)
-        for at in range(0, width, width // 2):
-            some = pl.ds(at, width // 2)
-            steps[i, some, :] = scale * jnp.dot(
-                proj_v[i, some, :], normalized[i], preferred_element_type=f32
-            )
-
-        pl.when(core == 0)(lambda: finish(i))
+            if turn_of == 0:
+                pl.when(~hub)(squares_in)
+            finish(i)
+
+        if turn_of == 0:
+            pl.when(me == 1)(squares_in)
 
     @pl.when(core == 1)
     def _():
         with jax.named_scope("fw"):
             arrived(weights.at[pl.ds(0, n - 1)], weight_at)
+        pl.when(me > 1)(squares_in)
         for i in range(2):
             finish(i)
 
     shard_size = 2 * rows * cols
     for c in range(half):
-        sent_pieces = 3 * half - 2
-        if half > 2:
-            sent_pieces += (c == 2) - (c == 0)
+        sent_pieces = 3 * half - 2 + (c == half // 2) - (c == 0)
         shards = [1 + direct_count(c)] * 2
         shards[0] += n - 2 + relay_count(c)
 
@@ -543,6 +563,7 @@
                 pltpu.VMEM((n, 2, cols), f32),
                 pltpu.VMEM((m, 2, cols), f32),
                 pltpu.VMEM((2, cols), f32),
+                pltpu.VMEM((2, cols), f32),
                 dma((2,)),
                 dma((len(CUTS) - 1,)),
                 dma,

time: 17.2 us -> 17 us (0.988)
  no operation moved by 1% of the time
where the time goes in v5:
time: 17 us; the launch traced here: 16.8 us
  Pallas kernels  16.2 us (95%)
  between operations  0.65 us (4%)
    pallas_call x1, Pallas kernels, body(): pl.pallas_call(functools.partial(exchange_kernel, n, m, float(rows * cols...  15.1 us
    pallas_call x1, Pallas kernels, body(): pl.pallas_call(store_kernel, out_shape=(sds((rows, cols), f32),) * 4 + (s...  1.07 us

profile of v5, /device:TPU:0, one launch (start us, length us, event | category | flops | bytes accessed | tf_op | source)
XLA Modules:
  0.0 16.8 jit_solution(7544592974105487328)
XLA Ops:
  0.6 15.1 %shard_map.186 = (f32[4,128,128]{2,1,0:T(8,128)S(1)}, f32[4,256,128]{2,1,0:T(8,128)S(1)}, bf16[2,1024,128]{2,1,0:T(8,128)(2,1)S(1)}) custom-call(bf16[2048,1024]{1,0:T(8,128)(2,1)} %latent.1, bf16[2048,128]{1,0:T(8,128)(2,1)} %key_cot.1, bf16[2048,128]{1,0:T(8,128)(2,1)} %value_cot.1, f32[128,128]{1,0:T(8,128)} %key_weight.1, f32[128,128]{1,0:T(8,128)} %value_weight.1, ...), custom_call_target="tpu_custom_call" | custom-call | tf_op jit(solution)/shard_map/pallas_call | solution.py:537
  15.8 1.1 %shard_map.187 = (f32[128,128]{1,0:T(8,128)}, f32[128,128]{1,0:T(8,128)}, f32[128,128]{1,0:T(8,128)}, f32[128,128]{1,0:T(8,128)}, f32[256,128]{1,0:T(8,128)}, /*...) custom-call(f32[4,128,128]{2,1,0:T(8,128)S(1)} %get-tuple-element.13, ...), custom_call_target="tpu_custom_call" | custom-call | tf_op jit(solution)/shard_map/pallas_call | solution.py:582

commit v6 on v5

--- a/solution.py
+++ b/solution.py
@@ -180,11 +180,11 @@
 
     piece_at, weight_at = recv_sem.at[0], recv_sem.at[1]
 
-    def join_at(i):
-        return recv_sem.at[2 + i]
+    def join_at(t):
+        return recv_sem.at[2 + t]
 
     def summed_at(owner, target):
-        return recv_sem.at[4 + slot(owner, target)]
+        return recv_sem.at[2 + half + slot(owner, target)]
 
     partner_at = recv_sem.at[0]
 
@@ -288,14 +288,20 @@
             arrived(squares, square_sem.at[1])
         set_scales()
 
+    urgent = (*range(1, half), 0)
     tail = jnp.where(chip == 0, half // 2, 0)
 
     @pl.when(core == 0)
     def _():
         for i in range(2):
-            part = pl.ds(i * rank, rank)
-            partial[part, :] = totals[i].astype(bf16).T
-            send(partial.at[part], joined.at[part], join_at(i), {"fs": partner})
+            partial[pl.ds(i * rank, rank), :] = totals[i].astype(bf16).T
+            for t in urgent:
+                if (1 if t == 0 else t * piece // rank) == i:
+                    part = pl.ds(t * piece, piece)
+                    send(
+                        partial.at[part], joined.at[part], join_at(t), {"fs": partner}
+                    )
+
         shift = jnp.where(chip == 1, 2, jnp.where(chip == half - 2, 1, 0))
         for k in range(half - 1):
             if k == 0:
@@ -355,24 +361,24 @@
     @pl.when(core == 1)
     def _():
         for i in range(2):
-            turned[i] = totals[i].T
-        for i in range(2):
-            part = pl.ds(i * rank, rank)
-            with jax.named_scope(f"join{i}"):
-                arrived(joined.at[part], join_at(i))
-            partial[part, :] = (turned[i] + joined[part, :].astype(f32)).astype(bf16)
-            for k in range(half - 1):
-                target = far_first(lax.rem(k + side, half - 1))
-                held_by = jnp.where(target == 0, 1, lax.div(target * piece, rank))
-
-                @pl.when(held_by == i)
-                def _():
-                    send(
-                        partial.at[pl.ds(target * piece, piece)],
-                        received.at[slot(chip, target)],
-                        piece_at,
-                        {"fs": 2 * target + 1},
-                    )
+            turned[pl.ds(i * rank, rank), :] = totals[i].T
+        for k, late in enumerate(urgent):
+            t = jnp.where((side == 0) & (late > 0), half - 1 - k, late)
+            part = pl.ds(pl.multiple_of(t * piece, piece), piece)
+            with jax.named_scope(f"join{k}"):
+                arrived(joined.at[part], join_at(t))
+            partial[part, :] = (turned[part, :] + joined[part, :].astype(f32)).astype(
+                bf16
+            )
+
+            @pl.when(chip != t)
+            def _():
+                send(
+                    partial.at[part],
+                    received.at[slot(chip, t)],
+                    piece_at,
+                    {"fs": 2 * t + 1},
+                )
 
         spread(1)
         with jax.named_scope("rs"):
@@ -381,7 +387,7 @@
         gathered[chip] = (
             own.astype(f32) + jnp.sum(received[...].astype(f32), axis=0)
         ).astype(bf16)
-        @pl.when(chip == half // 2)
+        @pl.when((chip == 1) | (chip == half // 2))
         def _():
             send(gathered.at[chip], gathered.at[chip], total_at(chip), {"fs": 0})
 
@@ -396,18 +402,22 @@
         send(gathered.at[chip], gathered.at[chip], total_at(chip), {"fs": partner})
         spread(2)
         for k in range(half - 1):
-            owner = near_first(jnp.where(chip == 1, (k + 1) % (half - 1), k))
+            place = jnp.where(chip == 0, half - 2 - k, k)
+            owner = near_first(jnp.where(chip == 1, (k + 1) % (half - 1), place))
 
             @pl.when(owner != tail)
             def _():
                 with jax.named_scope(f"ag{k}"):
                     arrived(gathered.at[owner], summed_at(owner, chip))
-                send(
-                    gathered.at[owner],
-                    gathered.at[owner],
-                    total_at(owner),
-                    {"fs": partner},
-                )
+
+                @pl.when((chip > 0) | (owner != 1))
+                def _():
+                    send(
+                        gathered.at[owner],
+                        gathered.at[owner],
+                        total_at(owner),
+                        {"fs": partner},
+                    )
 
     landed(moment_v, load_sem.at[1])
 
@@ -488,7 +498,8 @@
 
     shard_size = 2 * rows * cols
     for c in range(half):
-        sent_pieces = 3 * half - 2 + (c == half // 2) - (c == 0)
+        to_both = {1, half // 2}
+        sent_pieces = 3 * half - 2 + (c in to_both) - (c == 0) * len(to_both)
         shards = [1 + direct_count(c)] * 2
         shards[0] += n - 2 + relay_count(c)
 
@@ -555,7 +566,7 @@
                 pltpu.VMEM((2 * cols, width), bf16),
                 pltpu.VMEM((2 * rank, cols), bf16),
                 pltpu.VMEM((2 * rank, cols), bf16),
-                pltpu.VMEM((2, rank, cols), f32),
+                pltpu.VMEM((2 * rank, cols), f32),
                 pltpu.VMEM((2, n * rows, cols), f32),
                 pltpu.VMEM((2, rank, cols), bf16),
                 pltpu.VMEM((half - 1, piece, cols), bf16),

time: 17 us -> 16.9 us (level)
  Pallas kernels: 16.2 us -> 16 us
where the time goes in v6:
time: 16.9 us; the launch traced here: 16.7 us
  Pallas kernels  16 us (95%)
  between operations  0.65 us (4%)
    pallas_call x1, Pallas kernels, body(): pl.pallas_call(functools.partial(exchange_kernel, n, m, float(rows * cols...  15 us
    pallas_call x1, Pallas kernels, body(): pl.pallas_call(store_kernel, out_shape=(sds((rows, cols), f32),) * 4 + (s...  1.07 us

profile of v6, /device:TPU:0, one launch (start us, length us, event | category | flops | bytes accessed | tf_op | source)
XLA Modules:
  0.0 16.7 jit_solution(9116062517383193295)
XLA Ops:
  0.6 15.0 %shard_map.186 = (f32[4,128,128]{2,1,0:T(8,128)S(1)}, f32[4,256,128]{2,1,0:T(8,128)S(1)}, bf16[2,1024,128]{2,1,0:T(8,128)(2,1)S(1)}) custom-call(bf16[2048,1024]{1,0:T(8,128)(2,1)} %latent.1, bf16[2048,128]{1,0:T(8,128)(2,1)} %key_cot.1, bf16[2048,128]{1,0:T(8,128)(2,1)} %value_cot.1, f32[128,128]{1,0:T(8,128)} %key_weight.1, f32[128,128]{1,0:T(8,128)} %value_weight.1, ...), custom_call_target="tpu_custom_call" | custom-call | tf_op jit(solution)/shard_map/pallas_call | solution.py:548
  15.6 1.1 %shard_map.187 = (f32[128,128]{1,0:T(8,128)}, f32[128,128]{1,0:T(8,128)}, f32[128,128]{1,0:T(8,128)}, f32[128,128]{1,0:T(8,128)}, f32[256,128]{1,0:T(8,128)}, /*...) custom-call(f32[4,128,128]{2,1,0:T(8,128)S(1)} %get-tuple-element.13, ...), custom_call_target="tpu_custom_call" | custom-call | tf_op jit(solution)/shard_map/pallas_call | solution.py:593

commit v7 on v6

--- a/solution.py
+++ b/solution.py
@@ -387,10 +387,6 @@
         gathered[chip] = (
             own.astype(f32) + jnp.sum(received[...].astype(f32), axis=0)
         ).astype(bf16)
-        @pl.when((chip == 1) | (chip == half // 2))
-        def _():
-            send(gathered.at[chip], gathered.at[chip], total_at(chip), {"fs": 0})
-
         for k in range(half - 1):
             target = far_first(jnp.where(chip == 0, half - 2 - k, k))
             send(
@@ -399,6 +395,11 @@
                 summed_at(chip, target),
                 {"fs": 2 * target + 1},
             )
+
+            @pl.when((target == 0) & ((chip == 1) | (chip == half // 2)))
+            def _():
+                send(gathered.at[chip], gathered.at[chip], total_at(chip), {"fs": 0})
+
         send(gathered.at[chip], gathered.at[chip], total_at(chip), {"fs": partner})
         spread(2)
         for k in range(half - 1):

time: 16.9 us -> 17.2 us (1.018)
  Pallas kernels: 16 us -> 16.4 us
    pallas_call x1, Pallas kernels: 15 us -> 15.3 us  [body(): pl.pallas_call(functools.partial(exchange_kernel, n, m, float(rows * cols...]
where the time goes in v7:
time: 17.2 us; the launch traced here: 17 us
  Pallas kernels  16.4 us (95%)
  between operations  0.65 us (4%)
    pallas_call x1, Pallas kernels, body(): pl.pallas_call(functools.partial(exchange_kernel, n, m, float(rows * cols...  15.3 us
    pallas_call x1, Pallas kernels, body(): pl.pallas_call(store_kernel, out_shape=(sds((rows, cols), f32),) * 4 + (s...  1.07 us

profile of v7, /device:TPU:0, one launch (start us, length us, event | category | flops | bytes accessed | tf_op | source)
XLA Modules:
  0.0 17.0 jit_solution(12060461527978380510)
XLA Ops:
  0.6 15.3 %shard_map.186 = (f32[4,128,128]{2,1,0:T(8,128)S(1)}, f32[4,256,128]{2,1,0:T(8,128)S(1)}, bf16[2,1024,128]{2,1,0:T(8,128)(2,1)S(1)}) custom-call(bf16[2048,1024]{1,0:T(8,128)(2,1)} %latent.1, bf16[2048,128]{1,0:T(8,128)(2,1)} %key_cot.1, bf16[2048,128]{1,0:T(8,128)(2,1)} %value_cot.1, f32[128,128]{1,0:T(8,128)} %key_weight.1, f32[128,128]{1,0:T(8,128)} %value_weight.1, ...), custom_call_target="tpu_custom_call" | custom-call | tf_op jit(solution)/shard_map/pallas_call | solution.py:549
  16.0 1.1 %shard_map.187 = (f32[128,128]{1,0:T(8,128)}, f32[128,128]{1,0:T(8,128)}, f32[128,128]{1,0:T(8,128)}, f32[128,128]{1,0:T(8,128)}, f32[256,128]{1,0:T(8,128)}, /*...) custom-call(f32[4,128,128]{2,1,0:T(8,128)S(1)} %get-tuple-element.13, ...), custom_call_target="tpu_custom_call" | custom-call | tf_op jit(solution)/shard_map/pallas_call | solution.py:594
